TPU v7x, 256 devices: a whole 4x4x8 slice. The times are simulated.
256 devices in a mesh: sp: 32 (over z, x), tp: 8 (over y, core).
Axes of the slice: x: 4, y: 4, z: 8, core: 2. Of those that a mesh axis runs over, the one named last changes fastest.
Arguments:
- residual: bfloat16 [24576, 2048], P('sp'), may hold values from -6 to 6
- query_matrix: bfloat16 [24576, 1024], P('sp', 'tp'), may hold values from -6 to 6
- key_matrix: bfloat16 [24576, 1024], P('sp', 'tp'), may hold values from -6 to 6
- value_matrix: bfloat16 [24576, 2048], P('sp', 'tp'), may hold values from -6 to 6
- output_gate_logit: bfloat16 [24576, 2048], P('sp', 'tp'), may hold values from -6 to 6
- input_gate_log: float32 [24576, 8], P('sp', 'tp'), may hold values from -4 to 125
- forget_gate_logit: float32 [24576, 8], P('sp', 'tp')
- extra_head_decay: float32 [24576, 8], P('sp', 'tp'), may hold values from -1 to 0
- head_norm_gain: float32 [2048], P('tp'), may hold values from 0.1 to 1.9
- projection: bfloat16 [2048, 2048], P('tp'), may hold values from -5.303301 to 5.303301
- cell_output_gain: float32 [2048], replicated, may hold values from 0.1 to 1.9
- mixer_input_gain: float32 [2048], replicated, may hold values from 0.1 to 1.9
- mixer_gate_weight: bfloat16 [2048, 5120], P('sp', 'tp'), may hold values from -0.125 to 0.125
- mixer_up_weight: bfloat16 [2048, 5120], P('sp', 'tp'), may hold values from -0.125 to 0.125
- mixer_down_weight: bfloat16 [5120, 2048], P('tp', 'sp'), may hold values from -0.078125 to 0.078125
Outputs:
- updated: bfloat16 [24576, 2048], P('sp', 'tp')
All inputs are finite; a program needn't handle non-finite values.
Results may differ from a plain program's by a relative error of at most 0.014.
Values may be sent and summed in bfloat16 or wider, within the bound.
A program may use at most 128 MiB of HBM per device.

v0:
```python
import jax
import jax.numpy as jnp
from jax import lax
from jax.sharding import Mesh
from jax.sharding import PartitionSpec as P

DQK = 128
DV = 256
SP = ("sp_0", "sp_1")


HIGHEST = lax.Precision.HIGHEST
EPSILON = 1e-06
LOWEST_LOG = -1e30


def in_one_piece(arrays, axis, dim, along):
    both = jnp.concatenate(arrays, axis=along)
    whole, at, outs = (lax.all_gather(both, axis, axis=dim, tiled=True), 0, [])
    for a in arrays:
        outs.append(lax.slice_in_dim(whole, at, at + a.shape[along], axis=along))
        at += a.shape[along]
    return tuple(outs)


def from_everyone(value, axis):
    devices = lax.axis_size(axis)
    return lax.all_to_all(
        jnp.broadcast_to(value[None], (devices, *value.shape)), axis, 0, 0, tiled=True
    )


def joined_along(pieces, dim):
    pieces = jnp.moveaxis(pieces, 0, dim)
    dims = pieces.shape
    return pieces.reshape(*dims[:dim], dims[dim] * dims[dim + 1], *dims[dim + 2 :])


def collect(value, axis, dim):
    pieces = from_everyone(value, axis)
    return joined_along(pieces, dim)


def filled_with(value, identity):
    return jax.tree.map(
        lambda part, zero: jnp.zeros_like(part) + jnp.asarray(zero, part.dtype), value, identity
    )


def collected_together(value, axis):
    leaves = jax.tree.leaves(value)
    sequence = sorted(range(len(leaves)), key=lambda k: -leaves[k].size)
    width = (1, *leaves[sequence[0]].shape)[-1]
    lines = [
        jnp.pad(leaves[k].reshape(-1), (0, -leaves[k].size % width)).reshape(-1, width)
        for k in sequence
    ]
    both, at, found = (lax.all_gather(jnp.concatenate(lines), axis), 0, {})
    for k, line in zip(sequence, lines):
        slab = both[:, at : at + len(line)].reshape(len(both), -1)
        found[k] = slab[:, : leaves[k].size].reshape(-1, *leaves[k].shape)
        at += len(line)
    numbers = iter(range(len(leaves)))
    return jax.tree.map(lambda _: found[next(numbers)], value)


def prefix_by_axis(value, axes, combine, identity):
    before = start = filled_with(value, identity)
    subtotal = value
    for axis in reversed(axes):
        devices, place = (lax.axis_size(axis), lax.axis_index(axis))
        pieces = collected_together(subtotal, axis)
        inside, subtotal = (start, start)
        for k in range(devices):
            passed = k < place
            subtotal = combine(subtotal, jax.tree.map(lambda part: part[k], pieces))
            inside = jax.tree.map(lambda new, old: jnp.where(passed, new, old), subtotal, inside)
        before = combine(inside, before)
    return before


def heads_first(array, heads, width):
    return array.reshape(array.shape[0], heads, width).transpose(1, 0, 2)


def read_out(
    query_low, key_low, value_low, in_logs, running_log_total, memory, normalizer, stabilizer
):
    length = query_low.shape[1]
    causal = lax.broadcasted_iota(jnp.int32, (length, length), 0) >= lax.broadcasted_iota(
        jnp.int32, (length, length), 1
    )
    spread = running_log_total[:, :, None] - running_log_total[:, None, :] + in_logs[:, None, :]
    spread = jnp.where(causal[None], spread, -jnp.inf)
    carried = running_log_total + stabilizer[:, None]
    running = jnp.maximum(carried, jnp.max(spread, axis=-1))
    scores = jnp.einsum(
        "htd,hsd->hts", query_low, key_low, preferred_element_type=jnp.float32
    ) * DQK ** (-0.5)
    weights = jnp.exp(spread - running[:, :, None]) * scores
    scaled = jnp.exp(carried - running)
    scaled_query = query_low.astype(jnp.float32) * DQK ** (-0.5)
    numerator = jnp.einsum(
        "hts,hsv->htv", weights.astype(jnp.bfloat16), value_low, preferred_element_type=jnp.float32
    )
    numerator = numerator + scaled[:, :, None] * jnp.einsum(
        "hvd,htd->htv", memory, scaled_query, precision=HIGHEST
    )
    denominator = jnp.sum(weights, axis=-1) + scaled * jnp.einsum(
        "hd,htd->ht", normalizer, scaled_query, precision=HIGHEST
    )
    return numerator / jnp.maximum(jnp.abs(denominator), jnp.exp(-running))[:, :, None]


def fold_state(keyed, valued, in_logs, running_log_total, memory, normalizer, stabilizer):
    last = running_log_total[:, -1]
    lifted = last[:, None] - running_log_total + in_logs
    new_max = jnp.maximum(last + stabilizer, jnp.max(lifted, axis=-1))
    weights = jnp.exp(lifted - new_max[:, None])
    retained = jnp.exp(last + stabilizer - new_max)
    memory = retained[:, None, None] * memory + jnp.einsum(
        "hsv,hsd->hvd", weights[:, :, None] * valued, keyed, precision=HIGHEST
    )
    normalizer = retained[:, None] * normalizer + jnp.einsum(
        "hs,hsd->hd", weights, keyed, precision=HIGHEST
    )
    return (memory, normalizer, new_max)


def join_states(earlier, later):
    early_decay, early_memory, early_normalizer, early_max = earlier
    late_decay, late_memory, late_normalizer, late_max = later
    joined_max = jnp.maximum(late_decay + early_max, late_max)
    first_scale = jnp.exp(late_decay + early_max - joined_max)
    second_scale = jnp.exp(late_max - joined_max)
    memory = first_scale[:, None, None] * early_memory + second_scale[:, None, None] * late_memory
    normalizer = first_scale[:, None] * early_normalizer + second_scale[:, None] * late_normalizer
    return (early_decay + late_decay, memory, normalizer, joined_max)


def body(
    residual,
    query_matrix,
    key_matrix,
    value_matrix,
    output_gate_logit,
    input_gate_log,
    forget_gate_logit,
    extra_head_decay,
    head_norm_gain,
    projection,
    cell_output_gain,
    mixer_input_gain,
    mixer_gate_weight,
    mixer_up_weight,
    mixer_down_weight,
):
    gathered_in = in_one_piece((mixer_gate_weight, mixer_up_weight), SP, 0, 1)
    gathered_down = collect(mixer_down_weight, SP, 1)
    tok_rows = residual.shape[0]
    width = residual.shape[1]
    heads_here = input_gate_log.shape[1]
    query_low = heads_first(query_matrix, heads_here, DQK)
    key_low = heads_first(key_matrix, heads_here, DQK)
    value_low = heads_first(value_matrix, heads_here, DV)
    keyed = key_low.astype(jnp.float32)
    valued = value_low.astype(jnp.float32)
    in_logs = input_gate_log.T
    running_log_total = jnp.cumsum(
        (jax.nn.log_sigmoid(forget_gate_logit) + extra_head_decay).T, axis=-1
    )
    zero_memory = jnp.zeros((heads_here, DV, DQK), jnp.float32)
    zero_normalizer = jnp.zeros((heads_here, DQK), jnp.float32)
    lowest = jnp.full((heads_here,), LOWEST_LOG, jnp.float32)
    local_memory, local_normalizer, local_max = fold_state(
        keyed, valued, in_logs, running_log_total, zero_memory, zero_normalizer, lowest
    )
    prior_decay, prior_memory, prior_normalizer, prior_max = prefix_by_axis(
        (running_log_total[:, -1], local_memory, local_normalizer, local_max),
        SP,
        join_states,
        (jnp.zeros_like(lowest), zero_memory, zero_normalizer, lowest),
    )
    start_max = jnp.maximum(prior_decay, prior_max)
    lift = jnp.exp(prior_max - start_max)
    cells = read_out(
        query_low,
        key_low,
        value_low,
        in_logs,
        running_log_total,
        lift[:, None, None] * prior_memory,
        lift[:, None] * prior_normalizer,
        start_max,
    )
    centered = cells - jnp.mean(cells, axis=-1, keepdims=True)
    normed = centered * lax.rsqrt(jnp.mean(centered * centered, axis=-1, keepdims=True) + EPSILON)
    normed = normed * head_norm_gain.reshape(heads_here, DV)[:, None, :]
    normed = normed.transpose(1, 0, 2).reshape(tok_rows, heads_here * DV)
    gated = (normed * jax.nn.sigmoid(output_gate_logit.astype(jnp.float32))).astype(jnp.bfloat16)
    cols_here = width // lax.axis_size("tp")
    offset = lax.axis_index("tp") * cols_here
    mixed = lax.psum(
        jnp.dot(gated, projection, preferred_element_type=jnp.float32).astype(jnp.bfloat16), "tp"
    ).astype(jnp.float32)
    mixed = (
        mixed
        * lax.rsqrt(jnp.mean(mixed * mixed, axis=-1, keepdims=True) + EPSILON)
        * cell_output_gain
    )
    first_sum = (residual.astype(jnp.float32) + mixed).astype(jnp.bfloat16)
    first_wide = lax.optimization_barrier(first_sum).astype(jnp.float32)
    normed_rows = (
        first_wide
        * lax.rsqrt(jnp.mean(first_wide * first_wide, axis=-1, keepdims=True) + EPSILON)
        * mixer_input_gain
    ).astype(jnp.bfloat16)
    own_first = lax.dynamic_slice_in_dim(first_wide, offset, cols_here, 1)
    gate_value = jnp.dot(normed_rows, gathered_in[0], preferred_element_type=jnp.float32)
    up_value = jnp.dot(normed_rows, gathered_in[1], preferred_element_type=jnp.float32)
    activated = (jax.nn.silu(gate_value) * up_value).astype(jnp.bfloat16)
    down_terms = jnp.dot(activated, gathered_down, preferred_element_type=jnp.float32)
    channel_out = lax.psum_scatter(
        down_terms.astype(jnp.bfloat16), "tp", scatter_dimension=1, tiled=True
    ).astype(jnp.float32)
    return (own_first + 0.5 * channel_out).astype(jnp.bfloat16)


def solution(mesh):
    finer = Mesh(mesh.devices.reshape(8, 4, mesh.shape["tp"]), ("sp_0", "sp_1", "tp"))
    placed = (
        P(SP, None),
        P(SP, "tp"),
        P(SP, "tp"),
        P(SP, "tp"),
        P(SP, "tp"),
        P(SP, "tp"),
        P(SP, "tp"),
        P(SP, "tp"),
        P("tp"),
        P("tp", None),
        P(),
        P(),
        P(SP, "tp"),
        P(SP, "tp"),
        P("tp", SP),
    )
    return jax.shard_map(body, mesh=finer, in_specs=placed, out_specs=P(SP, "tp"), check_vma=False)
```

profile of v0, /device:TPU:1, one launch (start us, length us, event | category | flops | bytes accessed | tf_op | source)
XLA Modules:
  0.0 277.2 jit_solution(6400832605355430253)
XLA Ops:
  7.4 0.9 fusion.122
  9.6 1.9 fusion.119
  14.2 0.7 subtract_exponential_fusion.1
  14.9 1.8 fusion.16
  16.7 2.0 convolution_add_fusion
  18.7 12.3 %all-gather.2 = f32[4,259,128]{2,1,0:T(8,128)S(1)} all-gather(f32[1,259,128]{2,1,0:T(8,128)S(1)} %maximum_bitcast_fusion), channel_id=2, replica_groups=mesh['sp_0'=8,'sp_1'=4,'tp'=8] {'sp_1'}, dimensions={0}, use_global_device_ids=true | all-gather | bytes 663040 | tf_op jit(solution)/shard_map/all_gather | solution.py:58
  44.8 36.9 %all-gather.9.cloned.1.call-done = f32[8,259,128]{2,1,0:T(8,128)} async-done(((f32[1,259,128]{2,1,0:T(8,128)}), f32[8,259,128]{2,1,0:T(8,128)}) %all-gather.9.cloned.1.call-update) | async-done | bytes 1060880 | tf_op jit(solution)/shard_map/all_gather | solution.py:58
  81.8 0.8 fusion.193
  106.6 1.2 convolution_reduce_fusion
  107.9 2.4 fusion.200
  110.4 2.9 %convolution_convert_fusion.1 = bf16[768,2048]{1,0:T(8,128)(2,1)} fusion(bf16[256,2048]{1,0:T(8,128)(2,1)S(1)} %copy-done, bf16[768,256]{0,1:T(8,128)(2,1)S(1)} %copy.19, f32[768,256]{0,1:T(8,128)S(1)} %get-tuple-element.42, f32[256]{0:T(256)S(1)} %copy-done.12, f32[768]{0:T(1024)S(1)} %add_rsqrt_fusion.2, f32[768]{0:T(1024)S(1)} %broadcast_multiply_fusion), kind=kOutput, calls=%fused_computation.9 | convolution fusion | flops 808648704 | bytes 5381120 | tf_op jit(solution)/shard_map/dot_general | solution.py:204
  113.4 0.8 copy-done.6
  115.0 1.8 broadcast_in_dim.12
  116.8 7.3 %all-to-all-start = ((bf16[32,640,64]{1,2,0:T(8,128)(2,1)}), bf16[32,640,64]{1,2,0:T(8,128)(2,1)}, u32[]{:S(2)}, u32[]{:S(2)}) async-start(bf16[32,640,64]{1,2,0:T(8,128)(2,1)} %broadcast_in_dim.12), calls=%async_computation | async-start | bytes 5242880 | tf_op jit(solution)/shard_map/all_to_all | solution.py:28
  124.4 66.5 %all-reduce.6.cloned.1.call-done = bf16[768,2048]{1,0:T(8,128)(2,1)} async-done(((bf16[768,2048]{1,0:T(8,128)(2,1)}), bf16[768,2048]{1,0:T(8,128)(2,1)}) %all-reduce.6.cloned.1.call-update) | async-done | bytes 3145744 | tf_op jit(solution)/shard_map/psum | solution.py:203
  190.9 2.7 fusion
  193.8 3.8 %fusion.3 = bf16[768,2048]{1,0:T(8,128)(2,1)S(1)} fusion(bf16[768,2048]{1,0:T(8,128)(2,1)S(1)} %copy-done.2, bf16[768,2048]{1,0:T(8,128)(2,1)} %param.15, f32[2048]{0:T(1024)S(1)} %copy-done.9, f32[768]{0:T(1024)S(1)} %add_rsqrt_fusion.1), kind=kLoop, calls=%fused_computation.5 | loop fusion | flops 9437184 | bytes 9448448 | tf_op jit(solution)/shard_map/convert_element_type | solution.py:211
  197.6 1.7 copy-done.1
  200.0 14.9 %all-gather.7.cloned.1.call-done = bf16[2048,1280]{1,0:T(8,128)(2,1)} async-done(((bf16[64,1280]{1,0:T(8,128)(2,1)}), bf16[2048,1280]{1,0:T(8,128)(2,1)}) %all-gather.7.cloned.1.call-update) | async-done | bytes 5242896 | tf_op jit(solution)/shard_map/all_gather | solution.py:19
  214.9 5.3 %fusion.6 = f32[768,640]{1,0:T(8,128)S(1)} fusion(bf16[2048,1280]{1,0:T(8,128)(2,1)} %all-gather.7.cloned.1.call-done, f32[2048]{0:T(1024)S(1)} %copy-done.11, f32[768]{0:T(1024)S(1)} %add_rsqrt_fusion, bf16[768,2048]{1,0:T(8,128)(2,1)} %copy-done.1), kind=kOutput, calls=%fused_computation.12 | convolution fusion | flops 2019557376 | bytes 7744512 | tf_op jit(solution)/shard_map/dot_general | solution.py:219
  220.3 11.0 %convolution_convert_fusion = bf16[768,2048]{1,0:T(8,128)(2,1)} fusion(bf16[640,2048]{0,1:T(8,128)(2,1)} %bitcast.93, f32[768,640]{1,0:T(8,128)S(1)} %fusion.6, bf16[2048,1280]{1,0:T(8,128)(2,1)} %all-gather.7.cloned.1.call-done, f32[2048]{0:T(1024)S(1)} %copy-done.11, f32[768]{0:T(1024)S(1)} %add_rsqrt_fusion, bf16[768,2048]{1,0:T(8,128)(2,1)} %copy-done.1), kind=kOutput, calls=%fused_computation.8 | convolution fusion | flops 4037345280 | bytes 13511680 | tf_op jit(solution)/shard_map/dot_general | solution.py:222
  231.3 5.4 %convert_element_type.63 = f32[768,2048]{1,0:T(8,128)} convert(bf16[768,2048]{1,0:T(8,128)(2,1)} %copy-done.1) | non-fusion elementwise | flops 1572864 | bytes 9437184 | tf_op jit(solution)/shard_map/convert_element_type | solution.py:212
  236.7 31.3 %reduce-scatter.2.cloned.1.call-done = bf16[768,256]{1,0:T(8,128)(2,1)} async-done(((bf16[768,2048]{1,0:T(8,128)(2,1)}), bf16[768,256]{1,0:T(8,128)(2,1)}) %reduce-scatter.2.cloned.1.call-update) | async-done | bytes 393232 | tf_op jit(solution)/shard_map/reduce_scatter | solution.py:223
  268.0 2.1 add_convert_fusion
  (66 shorter events, 10.0 us)
Async XLA Ops:
  7.4 103.1 %copy-start = (bf16[256,2048]{1,0:T(8,128)(2,1)S(1)}, bf16[256,2048]{1,0:T(8,128)(2,1)}, u32[]{:S(2)}) copy-start(bf16[256,2048]{1,0:T(8,128)(2,1)} %param.24) | copy-start | bytes 3145732
  7.4 97.7 %copy-start.5 = (bf16[768,128]{1,0:T(8,128)(2,1)S(1)}, bf16[768,128]{1,0:T(8,128)(2,1)}, u32[]{:S(2)}) copy-start(bf16[768,128]{1,0:T(8,128)(2,1)} %param.17) | copy-start | bytes 589828
  7.4 36.9 %copy-start.4 = (bf16[768,256]{1,0:T(8,128)(2,1)S(1)}, bf16[768,256]{1,0:T(8,128)(2,1)}, u32[]{:S(2)}) copy-start(bf16[768,256]{1,0:T(8,128)(2,1)} %param.19) | copy-start | bytes 1179652
  7.4 97.7 %copy-start.10 = (bf16[768,128]{1,0:T(8,128)(2,1)S(1)}, bf16[768,128]{1,0:T(8,128)(2,1)}, u32[]{:S(2)}) copy-start(bf16[768,128]{1,0:T(8,128)(2,1)} %param.16) | copy-start | bytes 589828
  7.4 74.4 %all-gather.9.cloned.1.call-start = ((), (), s32[]{:S(2)}) async-start(), calls=%async_computation.5 | async-start | bytes 1216512 | tf_op jit(solution)/shard_map/all_gather | solution.py:58
  43.5 147.4 %all-reduce.6.cloned.1.call-start = ((), (), s32[]{:S(2)}) async-start(), calls=%async_computation.2 | async-start | bytes 6291456 | tf_op jit(solution)/shard_map/psum | solution.py:203
  105.1 1.0 copy-start.3
  107.9 2.6 copy-start.12
  113.3 0.9 copy-start.6
  113.3 0.9 copy-start.7
  113.3 1.6 copy-start.8
  113.4 101.5 %all-gather.7.cloned.1.call-start = ((), (), s32[]{:S(2)}) async-start(), calls=%async_computation.3 | async-start | bytes 5406720 | tf_op jit(solution)/shard_map/all_gather | solution.py:19
  116.8 103.4 %all-to-all-start = ((bf16[32,640,64]{1,2,0:T(8,128)(2,1)}), bf16[32,640,64]{1,2,0:T(8,128)(2,1)}, u32[]{:S(2)}, u32[]{:S(2)}) async-start(bf16[32,640,64]{1,2,0:T(8,128)(2,1)} %broadcast_in_dim.12), calls=%async_computation | async-start | bytes 5242880 | tf_op jit(solution)/shard_map/all_to_all | solution.py:28
  124.1 69.5 %copy-start.9 = (f32[2048]{0:T(1024)S(1)}, f32[2048]{0:T(1024)}, u32[]{:S(2)}) copy-start(f32[2048]{0:T(1024)} %param.25) | copy-start | bytes 24580
  124.2 143.9 %reduce-scatter.2.cloned.1.call-start = ((), (), s32[]{:S(2)}) async-start(), calls=%async_computation.4 | async-start | bytes 3538944 | tf_op jit(solution)/shard_map/reduce_scatter | solution.py:223
  190.9 2.9 %copy-start.2 = (bf16[768,2048]{1,0:T(8,128)(2,1)S(1)}, bf16[768,2048]{1,0:T(8,128)(2,1)}, u32[]{:S(2)}) copy-start(bf16[768,2048]{1,0:T(8,128)(2,1)} %all-reduce.6.cloned.1.call-done) | copy-start | bytes 9437188
  197.6 1.7 copy-start.1
  199.3 15.6 %copy-start.11 = (f32[2048]{0:T(1024)S(1)}, f32[2048]{0:T(1024)}, u32[]{:S(2)}) copy-start(f32[2048]{0:T(1024)} %param.26) | copy-start | bytes 24580
Sparse Core Ops, SparseCore 0:
  43.6 38.0 all-gather.8
  113.5 77.3 all-reduce.5
  231.4 36.5 reduce-scatter.1
Sparse Core Ops, SparseCore 1:
  116.4 98.4 all-gather.6
where the time goes:
time: 280 us; the launch traced here: 277 us
  waiting for transfers between devices  150 us (54%)
  between operations  48.6 us (17%)
  matrix products  27.9 us (10%)
  other arithmetic  21.2 us (8%)
  blocking collectives  12.3 us (4%)
  local copies, waits for them, and re-layouts  9.79 us (3%)
  starting transfers between devices  7.67 us (3%)
    psum x1, waiting for transfers between devices, body(): lax.psum(jnp.dot(gated, projection, preferred_element_type=jnp.float32).a...  66.5 us
    all_gather x1, waiting for transfers between devices, collected_together(): both, at, found = (lax.all_gather(jnp.concatenate(lines), axis), 0, {})  36.9 us
    reduce_scatter x1, waiting for transfers between devices, body(): lax.psum_scatter(down_terms.astype(jnp.bfloat16), 'tp', scatter_dimension...  31.3 us
    all_gather x1, waiting for transfers between devices, in_one_piece(): whole, at, outs = (lax.all_gather(both, axis, axis=dim, tiled=True), 0, [])  14.9 us
    all_gather x1, blocking collectives, collected_together(): both, at, found = (lax.all_gather(jnp.concatenate(lines), axis), 0, {})  12.3 us
    dot_general x1, matrix products, body(): jnp.dot(activated, gathered_down, preferred_element_type=jnp.float32)  11 us
    all_to_all x1, starting transfers between devices, from_everyone(): lax.all_to_all(jnp.broadcast_to(value[None], (devices, *value.shape)), ax...  7.33 us
  transfers between devices with their start and end apart: 5, of which 4 were waited for; matrix products, arithmetic and copies ran while one was open for 8% of the time, Pallas kernels for 0%

commit v1 on v0

v1 whole, which is shorter than its diff:
```python
import jax
import jax.numpy as jnp
from jax import lax
from jax.experimental import pallas as pl
from jax.experimental.pallas import tpu as pltpu
from jax.sharding import PartitionSpec as P

MESH = pl.DeviceIdType.MESH
F32, BF16 = jnp.float32, jnp.bfloat16
TOK, DQK, DV, WIDE, HID = 768, 128, 256, 2048, 640
NZ, NX, NY = 8, 4, 4
CUT = 768
ALL = 3 * HID
SCALE = DQK ** (-0.5)
EPSILON = 1e-06
LOW = -1e30
COPIES = 160


def dot(a, b):
    return lax.dot_general(a, b, (((1,), (0,)), ((), ())), preferred_element_type=F32)


def dot_nt(a, b):
    return lax.dot_general(a, b, (((1,), (1,)), ((), ())), preferred_element_type=F32)


def dot_tn(a, b):
    return lax.dot_general(a, b, (((0,), (0,)), ((), ())), preferred_element_type=F32)


class Wire:
    def __init__(self, send_sems, recv_sems):
        self.send_sems, self.recv_sems, self.open = send_sems, recv_sems, []

    def send(self, src, dst, to):
        k = len(self.open)
        copy = pltpu.make_async_remote_copy(
            src_ref=src,
            dst_ref=dst,
            send_sem=self.send_sems.at[k],
            recv_sem=self.recv_sems.at[k],
            device_id=to,
            device_id_type=MESH,
        )
        copy.start()
        self.open.append(copy)
        return copy


def rows_at(start, size, unit):
    return pl.ds(pl.multiple_of(start, unit), size)


def blocks(count, step):
    def run(i, carry):
        step(i)
        return carry

    lax.fori_loop(0, count, run, 0)


def layer(
    fg, ig, dec, hg, cg, mg,
    q_h, k_h, v_h, og_h, proj_h, res_h, wg_h, wu_h, wd_h,
    out,
    gates, rows_t, cols_t, acol, gcol, bcol,
    q, k, v, og, proj, res, w_all,
    num, den,
    st_own, st_row, ax_own, ax_row, sub, st_col, ax_sub, ax_col, st_out, st_prior,
    gated, part, part_sib, pair, ring, ring_sum,
    first, rows_n, hid, act,
    down, down_sib, pair2, ring2, ring2_sum,
    local_sems, send_sems, recv_sems,
):
    sp, tp = lax.axis_index("sp"), lax.axis_index("tp")
    z, x = sp // NX, lax.rem(sp, NX)
    y, c = tp // 2, lax.rem(tp, 2)
    wire = Wire(send_sems, recv_sems)

    def at(dz=0, dx=0, dy=0, flip=False):
        zz, xx = lax.rem(z + dz, NZ), lax.rem(x + dx, NX)
        yy, cc = lax.rem(y + dy, NY), (1 - c if flip else c)
        return (zz * NX + xx, yy * 2 + cc)

    sibling = at(flip=True)
    up_y, down_y = at(dy=1), at(dy=NY - 1)
    up_z, down_z = at(dz=1), at(dz=NZ - 1)
    up_x, down_x = at(dx=1), at(dx=NX - 1)

    own_w = rows_at(64 * sp, 64, 64)
    plan = [
        (wg_h, w_all.at[own_w, 0:HID]),
        (wu_h, w_all.at[own_w, HID : 2 * HID]),
        (wd_h, w_all.at[own_w, 2 * HID : 3 * HID]),
        (k_h, k),
        (v_h, v),
        (q_h, q),
        (og_h, og),
        (proj_h, proj),
        (res_h.at[rows_at(96 * tp, 96, 32), :], res),
    ]
    loads = [
        pltpu.make_async_copy(src, dst, local_sems.at[i]) for i, (src, dst) in enumerate(plan)
    ]
    for load in loads:
        load.start()
    load_w, (load_k, load_v, load_q, load_og, load_proj, load_res) = loads[:3], loads[3:]

    barrier = pltpu.get_barrier_semaphore()
    peers = [sibling, up_y, down_y]
    peers += [at(dz=o) for o in range(1, NZ)] + [at(dx=o) for o in range(1, NX)]
    for peer in peers:
        pl.semaphore_signal(barrier, inc=1, device_id=peer, device_id_type=MESH)

    lane = lax.broadcasted_iota(jnp.int32, (8, 128), 1)
    subl = lax.broadcasted_iota(jnp.int32, (8, 128), 0)

    def scan(value, op, identity):
        for shift in (1, 2, 4, 8, 16, 32, 64):
            moved = pltpu.roll(value, shift, axis=1)
            value = op(value, jnp.where(lane >= shift, moved, identity))
        total = jnp.broadcast_to(value[:, 127:128], (8, 128))
        for shift in (1, 2, 4):
            moved = pltpu.roll(total, shift, axis=0)
            total = op(total, jnp.where(subl >= shift, moved, identity))
        before = jnp.where(subl >= 1, pltpu.roll(total, 1, axis=0), identity)
        return op(value, before)

    for i, ref in enumerate((fg, ig, dec)):
        gates[i] = jnp.zeros((8, 128), F32)
        for r in range(6):
            gates[i, r : r + 1, :] = ref[0:1, 128 * r : 128 * (r + 1)]
    logit = gates[0]
    forget = jnp.minimum(logit, 0.0) - jnp.log1p(jnp.exp(-jnp.abs(logit))) + gates[2]
    total_log = scan(forget, jnp.add, 0.0)
    a_rows = gates[1] - total_log
    peak = scan(a_rows, jnp.maximum, LOW)
    decay_own = total_log[5:6, 127:128]
    a_max = peak[5:6, 127:128]
    rows_t[0:8, :] = a_rows
    rows_t[8:16, :] = peak
    rows_t[16:24, :] = total_log
    rows_t[24:128, :] = jnp.zeros((104, 128), F32)
    cols_t[...] = jnp.transpose(rows_t[...])
    for r in range(6):
        here = slice(128 * r, 128 * (r + 1))
        acol[here, :] = cols_t[:, r : r + 1]
        gcol[here, :] = cols_t[:, 8 + r : 9 + r]
        bcol[here, :] = cols_t[:, 16 + r : 17 + r]

    pl.semaphore_wait(barrier, len(peers))

    def piece(dz, dx, rows=64, skip=0):
        zz, xx = lax.rem(z + dz, NZ), lax.rem(x + dx, NX)
        return rows_at(64 * (NX * zz + xx) + skip, rows, 32)

    def run(dz, rows=256, skip=0):
        return rows_at(256 * lax.rem(z + dz, NZ) + skip, rows, 128)

    LEFT, RIGHT = slice(0, CUT), slice(CUT, ALL)

    def send_w(rows, cols, to):
        return wire.send(w_all.at[rows, cols], w_all.at[rows, cols], to)

    def a2(s):
        half = 128 if s == 4 else 256
        return (
            send_w(run(NZ + 1 - s, half), LEFT, up_z),
            send_w(run(s - 1, half, 256 - half), LEFT, down_z),
        )

    def b1(s):
        half = 32 if s == 4 else 64
        return (
            send_w(piece(NZ + 1 - s, 0, half), RIGHT, up_z),
            send_w(piece(s - 1, 0, half, 64 - half), RIGHT, down_z),
        )

    def b2(dz):
        return (send_w(piece(dz, 0), RIGHT, up_x), send_w(piece(dz, 0), RIGHT, down_x))

    def onward_up(dz):
        return send_w(piece(dz, NX - 1), RIGHT, up_x)

    def onward_down(dz):
        return send_w(piece(dz, 1), RIGHT, down_x)

    def landed(copies):
        for copy in copies:
            copy.wait_recv()

    for load in load_w:
        load.wait()
    A1 = [send_w(piece(0, 0), LEFT, at(dx=o)) for o in (1, 3, 2)]
    A2, B1, B2, ON = {}, {}, {}, {}
    B1[1] = b1(1)

    load_k.wait()
    load_v.wait()
    state = jnp.zeros((DQK, DV), F32)
    norm = jnp.zeros((1, DQK), F32)
    for i in range(3):
        here = slice(256 * i, 256 * (i + 1))
        lift = jnp.exp(acol[here, :] - a_max)
        keys = k[here, :]
        state = state + dot_tn(keys, (lift * v[here, :].astype(F32)).astype(BF16))
        norm = norm + jnp.sum(lift * keys.astype(F32), axis=0, keepdims=True)

    def wide(value):
        return jnp.broadcast_to(value, (1, 128))

    for j in range(NX):
        st_own[j] = state[32 * j : 32 * (j + 1), :].astype(BF16)
    ax_own[...] = jnp.concatenate(
        [norm, wide(decay_own), wide(decay_own + a_max), jnp.zeros((5, 128), F32)], axis=0
    )
    S1 = []
    for o in range(1, NX):
        S1.append(wire.send(st_own.at[lax.rem(x + o, NX)], st_row.at[x], at(dx=o)))
        S1.append(wire.send(ax_own, ax_row.at[x], at(dx=o)))
    st_row[x] = st_own[x]
    ax_row[x] = ax_own[...]
    B2[0] = b2(0)

    load_q.wait()
    diagonal = lax.broadcasted_iota(jnp.int32, (256, 256), 0) >= lax.broadcasted_iota(
        jnp.int32, (256, 256), 1
    )

    def attend(i):
        here = slice(256 * i, 256 * (i + 1))
        queries = q[here, :]
        top = gcol[here, :]
        over = jnp.zeros((256, DV), F32)
        under = jnp.zeros((256, 1), F32)
        for j in range(i + 1):
            there = slice(256 * j, 256 * (j + 1))
            a_line = jnp.concatenate(
                [rows_t[2 * j : 2 * j + 1, :], rows_t[2 * j + 1 : 2 * j + 2, :]], axis=1
            )
            power = a_line - top
            if i == j:
                power = jnp.where(diagonal, power, LOW)
            weight = jnp.exp(power) * (dot_nt(queries, k[there, :]) * SCALE)
            under = under + jnp.sum(weight, axis=1, keepdims=True)
            over = over + dot(weight.astype(BF16), v[there, :])
        num[here, :] = over
        den[here, :] = under

    attend(0)
    landed(A1)
    A2[1] = a2(1)

    landed(S1)
    decay = [ax_row[i, 1:2, :] for i in range(NX)]
    peaks = [ax_row[i, 2:3, :] for i in range(NX)]
    norms = [ax_row[i, 0:1, :] for i in range(NX)]

    def between(i, j):
        total = jnp.zeros((1, 128), F32)
        for m in range(i + 1, j):
            total = total + decay[m]
        return total

    tops = [peaks[i] + between(i, NX) for i in range(NX)]
    row_peak = jnp.maximum(jnp.maximum(tops[0], tops[1]), jnp.maximum(tops[2], tops[3]))
    gains = [jnp.exp(top - row_peak) for top in tops]
    row_state = sum(gains[i][:, 0:1] * st_row[i].astype(F32) for i in range(NX))
    row_norm = sum(gains[i] * norms[i] for i in range(NX))
    sub[...] = row_state.astype(BF16)
    ax_sub[...] = jnp.concatenate(
        [row_norm, between(-1, NX), row_peak, jnp.zeros((5, 128), F32)], axis=0
    )
    S2 = []
    for o in (4, 3, 5, 2, 6, 1, 7):
        S2.append(wire.send(sub, st_col.at[z], at(dz=o)))
        S2.append(wire.send(ax_sub, ax_col.at[z], at(dz=o)))
    st_col[z] = sub[...]
    ax_col[z] = ax_sub[...]

    landed(B1[1])
    B1[2] = b1(2)
    B2[1], B2[7] = b2(1), b2(NZ - 1)
    attend(1)
    attend(2)

    landed(S2)
    col_peak = jnp.full((1, 128), LOW, F32)
    col_decay = jnp.zeros((1, 128), F32)
    col_norm = jnp.zeros((1, 128), F32)
    col_state = jnp.zeros((32, DV), F32)
    for zz in range(NZ - 1):
        passed = zz < z
        late_decay, late_peak = ax_col[zz, 1:2, :], ax_col[zz, 2:3, :]
        joined = jnp.maximum(late_decay + col_peak, late_peak)
        f1 = jnp.where(passed, jnp.exp(late_decay + col_peak - joined), 1.0)
        f2 = jnp.where(passed, jnp.exp(late_peak - joined), 0.0)
        col_state = f1[:, 0:1] * col_state + f2[:, 0:1] * st_col[zz].astype(F32)
        col_norm = f1 * col_norm + f2 * ax_col[zz, 0:1, :]
        col_decay = jnp.where(passed, col_decay + late_decay, col_decay)
        col_peak = jnp.where(passed, joined, col_peak)

    start = jnp.zeros((1, 128), F32)
    prior_norm = jnp.zeros((1, 128), F32)
    for t in range(NX):
        row_decay = between(-1, t)
        highest = row_decay + jnp.maximum(col_peak, col_decay)
        for i in range(t):
            highest = jnp.maximum(highest, peaks[i] + between(i, t))
        f0 = jnp.exp(row_decay + col_peak - highest)
        joint, joint_norm = f0[:, 0:1] * col_state, f0 * col_norm
        for i in range(t):
            f = jnp.exp(peaks[i] + between(i, t) - highest)
            joint = joint + f[:, 0:1] * st_row[i].astype(F32)
            joint_norm = joint_norm + f * norms[i]
        st_out[t] = joint.astype(BF16)
        start = jnp.where(x == t, highest, start)
        prior_norm = jnp.where(x == t, joint_norm, prior_norm)
    S3 = [
        wire.send(st_out.at[lax.rem(x + o, NX)], st_prior.at[x], at(dx=o)) for o in range(1, NX)
    ]
    st_prior[x] = st_out[x]
    landed(A2[1])
    A2[2] = a2(2)
    landed(B2[0])
    ON[0] = onward_up(0)
    load_og.wait()
    load_proj.wait()
    load_res.wait()

    landed(S3)
    prior = st_prior[...].reshape(DQK, DV)
    start = start[:, 0:1]

    def finish_cell(i):
        here = slice(256 * i, 256 * (i + 1))
        own_top = gcol[here, :]
        top = jnp.maximum(own_top, start)
        keep = jnp.exp(own_top - top)
        carry = jnp.exp(start - top) * SCALE
        queries = q[here, :]
        over = keep * num[here, :] + carry * dot(queries, prior)
        under = keep * den[here, :] + carry * jnp.sum(
            queries.astype(F32) * prior_norm, axis=1, keepdims=True
        )
        floor = jnp.exp(-(bcol[here, :] + top))
        cell = over / jnp.maximum(jnp.abs(under), floor)
        centred = cell - jnp.mean(cell, axis=1, keepdims=True)
        spread = jnp.mean(centred * centred, axis=1, keepdims=True)
        normed = centred * lax.rsqrt(spread + EPSILON) * hg[...]
        gated[here, :] = (normed * jax.nn.sigmoid(og[here, :].astype(F32))).astype(BF16)

    for i in range(3):
        finish_cell(i)
    landed(B1[2])
    B1[3] = b1(3)
    B2[2], B2[6] = b2(2), b2(NZ - 2)

    def project(o):
        yy = lax.rem(y + o, NY)
        here = rows_at(192 * yy, 192, 64)
        left = gated[here, :]
        for n in range(8):
            cols = slice(256 * n, 256 * (n + 1))
            part[here, cols] = dot(left, proj[:, cols]).astype(BF16)
        theirs = rows_at(96 * (2 * yy + 1 - c), 96, 32)
        return wire.send(part.at[theirs, :], part_sib.at[o], sibling)

    def pair_up(o):
        yy = lax.rem(y + o, NY)

        def step(i):
            mine = rows_at(96 * (2 * yy + c) + 16 * i, 16, 16)
            here = rows_at(16 * i, 16, 16)
            total = part[mine, :].astype(F32) + part_sib[o, here, :].astype(F32)
            pair[o, here, :] = total.astype(BF16)

        blocks(6, step)

    H0, H1 = slice(0, 48), slice(48, 96)
    D = {}
    D[2] = project(2)
    D[1] = project(1)
    landed([D[2]])
    pair_up(2)
    M1 = wire.send(pair.at[2, H0, :], ring.at[0], up_y)
    M1b = wire.send(pair.at[2, H1, :], ring.at[1], down_y)
    D[3] = project(3)
    landed([D[1]])
    pair_up(1)
    M2 = wire.send(pair.at[1, H1, :], ring.at[2], up_y)
    D[0] = project(0)
    landed([D[3]])
    pair_up(3)
    M2b = wire.send(pair.at[3, H0, :], ring.at[3], down_y)

    landed(A2[2])
    A2[3] = a2(3)
    landed(B2[1] + B2[7])
    ON[7] = onward_up(NZ - 1)
    ON[1] = onward_down(1)

    landed([D[0]])
    pair_up(0)

    def ring_add(o, skip, slot, into):
        def step(i):
            here = rows_at(16 * i, 16, 16)
            there = rows_at(16 * i + skip, 16, 16)
            total = pair[o, there, :].astype(F32) + ring[slot, here, :].astype(F32)
            ring_sum[into, here, :] = total.astype(BF16)

        blocks(3, step)

    landed([M1])
    ring_add(1, 0, 0, 0)
    M3 = wire.send(ring_sum.at[0], ring.at[4], up_y)
    landed([M1b])
    ring_add(3, 48, 1, 1)
    M3b = wire.send(ring_sum.at[1], ring.at[5], down_y)

    landed(B1[3])
    B1[4] = b1(4)
    B2[3], B2[5] = b2(3), b2(NZ - 3)
    landed(B2[2] + B2[6])
    ON[6] = onward_up(NZ - 2)
    ON[2] = onward_down(2)

    own_first = 96 * tp

    def finish_mix(skip, one, two):
        def step(i):
            here = rows_at(16 * i, 16, 16)
            there = rows_at(16 * i + skip, 16, 16)
            mix = (
                pair[0, there, :].astype(F32)
                + ring[one, here, :].astype(F32)
                + ring[two, here, :].astype(F32)
            )
            scale = lax.rsqrt(jnp.mean(mix * mix, axis=1, keepdims=True) + EPSILON)
            total = res[there, :].astype(F32) + mix * scale * cg[...]
            first[rows_at(own_first + skip + 16 * i, 16, 16), :] = total.astype(BF16)

        blocks(3, step)

    def first_rows(dy, half, cc):
        return rows_at(96 * (2 * lax.rem(y + dy, NY) + cc) + 48 * half, 48, 16)

    def share(dy, half, to):
        rows = first_rows(dy, half, c)
        return wire.send(first.at[rows, :], first.at[rows, :], to)

    landed([M3, M2b])
    finish_mix(0, 4, 3)
    N1, N2b, E0 = share(0, 0, up_y), share(0, 0, down_y), share(0, 0, sibling)
    landed([M2, M3b])
    finish_mix(48, 2, 5)
    N2, N1b, E1 = share(0, 1, up_y), share(0, 1, down_y), share(0, 1, sibling)

    landed(A2[3])
    A2[4] = a2(4)
    landed(B1[4])
    B2[4] = b2(4)
    landed(B2[3] + B2[5])
    ON[5] = onward_up(NZ - 3)
    ON[3] = onward_down(3)

    landed([N1])
    N3, E2 = share(3, 0, up_y), share(3, 0, sibling)
    landed([N1b])
    N3b, E3 = share(1, 1, down_y), share(1, 1, sibling)

    landed(B2[4])
    ON[4] = onward_down(4)
    landed([N2])
    E4 = share(3, 1, sibling)
    landed([N2b])
    E5 = share(1, 0, sibling)
    landed(A2[4])
    for s in range(NZ):
        landed([ON[s]])

    def mixer(o):
        yy = lax.rem(y + o, NY)

        def normalise(i):
            rows = first[rows_at(192 * yy + 16 * i, 16, 16), :].astype(F32)
            scale = lax.rsqrt(jnp.mean(rows * rows, axis=1, keepdims=True) + EPSILON)
            rows_n[rows_at(16 * i, 16, 16), :] = (rows * scale * mg[...]).astype(BF16)

        blocks(12, normalise)

        def widen(i):
            cols = pl.ds(pl.multiple_of(256 * i, 256), 256)
            hid[:, cols] = dot(rows_n[...], w_all[:, cols])

        blocks(5, widen)

        def activate(i):
            here = rows_at(16 * i, 16, 16)
            gate, value = hid[here, 0:HID], hid[here, HID : 2 * HID]
            act[here, :] = (gate * jax.nn.sigmoid(gate) * value).astype(BF16)

        blocks(12, activate)

        def narrow(cc):
            def step(i):
                rows = rows_at(256 * (2 * i + cc), 256, 256)
                total = dot_nt(act[...], w_all[rows, 2 * HID : 3 * HID])
                down[o, cc, i] = total.astype(BF16)

            blocks(4, step)

        narrow(1 - c)
        theirs = wire.send(down.at[o, 1 - c], down_sib.at[o], sibling)
        narrow(c)
        return theirs

    G, G1, G1b, G2, G2b, G3, G3b = {}, {}, {}, {}, {}, {}, {}

    def group(o):
        return lax.rem(y + o, NY)

    L0, L1 = slice(0, 96), slice(96, 192)

    def spread_out(o):
        landed([G[o]])

        def add(p):
            yy = lax.rem(y + p, NY)

            def step(i):
                here = rows_at(32 * i, 32, 32)
                total = down[o, c, yy, here, :].astype(F32) + down_sib[o, yy, here, :].astype(F32)
                pair2[o, p, here, :] = total.astype(BF16)

            blocks(6, step)

        add(2)
        G1[o] = wire.send(pair2.at[o, 2, L0, :], ring2.at[group(o), 0], up_y)
        G1b[o] = wire.send(pair2.at[o, 2, L1, :], ring2.at[group(o), 1], down_y)
        add(1)
        G2[o] = wire.send(pair2.at[o, 1, L1, :], ring2.at[group(o), 2], up_y)
        add(3)
        G2b[o] = wire.send(pair2.at[o, 3, L0, :], ring2.at[group(o), 3], down_y)
        add(0)

    def ring2_add(o, p, skip, slot, into):
        def step(i):
            here = rows_at(32 * i, 32, 32)
            there = rows_at(32 * i + skip, 32, 32)
            total = pair2[o, p, there, :].astype(F32) + ring2[group(o), slot, here, :].astype(F32)
            ring2_sum[o, into, here, :] = total.astype(BF16)

        blocks(3, step)

    def pass_up(o):
        landed([G1[(o + 1) % NY]])
        ring2_add(o, 1, 0, 0, 0)
        G3[o] = wire.send(ring2_sum.at[o, 0], ring2.at[group(o), 4], up_y)

    def pass_down(o):
        landed([G1b[(o + 3) % NY]])
        ring2_add(o, 3, 96, 1, 1)
        G3b[o] = wire.send(ring2_sum.at[o, 1], ring2.at[group(o), 5], down_y)

    landed([E0, E1])
    G[0] = mixer(0)
    spread_out(0)
    landed([N3])
    E6 = share(2, 0, sibling)
    landed([N3b])
    E7 = share(2, 1, sibling)
    landed([E3, E5])
    G[1] = mixer(1)
    spread_out(1)
    landed([E2, E4])
    G[3] = mixer(3)
    spread_out(3)
    landed([E6, E7])
    G[2] = mixer(2)
    spread_out(2)
    for o_up, o_down in ((3, 1), (0, 2), (2, 0), (1, 3)):
        pass_up(o_up)
        pass_down(o_down)

    own_cols = pl.ds(pl.multiple_of(DV * tp, DV), DV)

    def finish(o, skip, one, two):
        def step(i):
            here = rows_at(32 * i, 32, 32)
            there = rows_at(32 * i + skip, 32, 32)
            rows = rows_at(192 * group(o) + skip + 32 * i, 32, 32)
            total = (
                pair2[o, 0, there, :].astype(F32)
                + ring2[group(o), one, here, :].astype(F32)
                + ring2[group(o), two, here, :].astype(F32)
            )
            out[rows, :] = (first[rows, own_cols].astype(F32) + 0.5 * total).astype(BF16)

        blocks(3, step)

    for o in (0, 3, 1, 2):
        landed([G3[(o + 1) % NY], G2b[(o + 3) % NY]])
        finish(o, 0, 4, 3)
        landed([G2[(o + 1) % NY], G3b[(o + 3) % NY]])
        finish(o, 96, 2, 5)

    for copy in wire.open:
        copy.wait_send()


def body(
    residual, query, key, value, gate_logit, in_gate, forget_logit, decay,
    head_gain, projection, cell_gain, mixer_gain, gate_w, up_w, down_w,
):
    line = lambda a: a.reshape(1, -1)
    vmem = lambda *dims: pltpu.VMEM(dims, BF16)
    wide = lambda *dims: pltpu.VMEM(dims, F32)
    scratch = [
        wide(3, 8, 128), wide(128, 128), wide(128, 128),
        wide(TOK, 1), wide(TOK, 1), wide(TOK, 1),
        vmem(TOK, DQK), vmem(TOK, DQK), vmem(TOK, DV), vmem(TOK, DV),
        vmem(DV, WIDE), vmem(96, WIDE), vmem(WIDE, ALL),
        wide(TOK, DV), wide(TOK, 1),
        vmem(NX, 32, DV), vmem(NX, 32, DV), wide(8, 128), wide(NX, 8, 128),
        vmem(32, DV), vmem(NZ, 32, DV), wide(8, 128), wide(NZ, 8, 128),
        vmem(NX, 32, DV), vmem(NX, 32, DV),
        vmem(TOK, DV), vmem(TOK, WIDE), vmem(NY, 96, WIDE), vmem(NY, 96, WIDE),
        vmem(6, 48, WIDE), vmem(2, 48, WIDE),
        vmem(TOK, WIDE), vmem(192, WIDE), wide(192, 2 * HID), vmem(192, HID),
        vmem(NY, 2, NY, 192, DV), vmem(NY, NY, 192, DV), vmem(NY, NY, 192, DV),
        vmem(NY, 6, 96, DV), vmem(NY, 2, 96, DV),
        pltpu.SemaphoreType.DMA((9,)),
        pltpu.SemaphoreType.DMA((COPIES,)),
        pltpu.SemaphoreType.DMA((COPIES,)),
    ]
    in_vmem = pl.BlockSpec(memory_space=pltpu.VMEM)
    in_hbm = pl.BlockSpec(memory_space=pltpu.HBM)
    return pl.pallas_call(
        layer,
        out_shape=jax.ShapeDtypeStruct((TOK, DV), BF16),
        in_specs=[in_vmem] * 6 + [in_hbm] * 9,
        out_specs=in_vmem,
        scratch_shapes=scratch,
        compiler_params=pltpu.CompilerParams(
            collective_id=0, has_side_effects=True, vmem_limit_bytes=60 * 1024 * 1024
        ),
    )(
        line(forget_logit), line(in_gate), line(decay),
        line(head_gain), line(cell_gain), line(mixer_gain),
        query, key, value, gate_logit, projection, residual, gate_w, up_w, down_w.T,
    )


def solution(mesh):
    placed = (
        P("sp", None), P("sp", "tp"), P("sp", "tp"), P("sp", "tp"), P("sp", "tp"),
        P("sp", "tp"), P("sp", "tp"), P("sp", "tp"),
        P("tp"), P("tp", None), P(), P(),
        P("sp", "tp"), P("sp", "tp"), P("tp", "sp"),
    )
    return jax.shard_map(body, mesh=mesh, in_specs=placed, out_specs=P("sp", "tp"), check_vma=False)
```

time: 280 us -> 110 us (0.39); the launches traced: 277 us -> 110 us
  waiting for transfers between devices: 150 us -> 0 us
  Pallas kernels: 0 us -> 108 us
  between operations: 48.6 us -> 0.01 us
  matrix products: 27.9 us -> 0 us
  other arithmetic: 21.2 us -> 0 us
  blocking collectives: 12.3 us -> 0 us
  local copies, waits for them, and re-layouts: 9.79 us -> 1.77 us
  starting transfers between devices: 7.67 us -> 0 us
    pallas_call x0 -> x1, Pallas kernels: none -> 108 us  [body(): pl.pallas_call(layer, out_shape=jax.ShapeDtypeStruct((TOK, DV), BF16), in...]
    psum x1 -> x0, waiting for transfers between devices: 66.5 us -> none  [body(): lax.psum(jnp.dot(gated, projection, preferred_element_type=jnp.float32).a...]
    all_gather x2 -> x0, waiting for transfers between devices: 51.8 us -> none  [the longest x1 36.9 us: collected_together(): both, at, found = (lax.all_gather(jnp.concatenate(lines), axis), 0, {})]
    reduce_scatter x1 -> x0, waiting for transfers between devices: 31.3 us -> none  [body(): lax.psum_scatter(down_terms.astype(jnp.bfloat16), 'tp', scatter_dimension...]
    dot_general x9 -> x0, matrix products: 27.9 us -> none  [the longest x1 11 us: body(): jnp.dot(activated, gathered_down, preferred_element_type=jnp.float32)]
    all_gather x1 -> x0, blocking collectives: 12.3 us -> none  [collected_together(): both, at, found = (lax.all_gather(jnp.concatenate(lines), axis), 0, {})]
    convert_element_type x3 -> x0, other arithmetic: 11.3 us -> none  [the longest x1 5.4 us: body(): first_wide = lax.optimization_barrier(first_sum).astype(jnp.float32)]
    all_to_all x1 -> x0, starting transfers between devices: 7.33 us -> none  [from_everyone(): lax.all_to_all(jnp.broadcast_to(value[None], (devices, *value.shape)), ax...]
  transfers between devices with their start and end apart: 5 -> 0, of which waited for: 4 -> 0; matrix products, arithmetic and copies ran while one was open for 8% -> 0% of each run, Pallas kernels for 0% -> 0%
where the time goes in v1:
time: 110 us
  Pallas kernels  108 us (98%)
  local copies, waits for them, and re-layouts  1.77 us (2%)
    pallas_call x1, Pallas kernels, body(): pl.pallas_call(layer, out_shape=jax.ShapeDtypeStruct((TOK, DV), BF16), in...  108 us

profile of v1, /device:TPU:1, one launch (start us, length us, event | category | flops | bytes accessed | tf_op | source)
XLA Modules:
  0.0 110.1 jit_solution(15241796987200176948)
XLA Ops:
  0.0 108.3 %shard_map.145 = bf16[768,256]{1,0:T(8,128)(2,1)} custom-call(f32[1,768]{1,0:T(1,128)} %bitcast.10, f32[1,768]{1,0:T(1,128)} %bitcast.11, f32[1,768]{1,0:T(1,128)} %bitcast.12, f32[1,256]{1,0:T(1,128)} %bitcast.13, f32[1,2048]{1,0:T(1,128)} %bitcast.8, f32[1,2048]{1,0:T(1,128)} %bitcast.9, bf16[768,128]{1,0:T(8,128)(2,1)} %q_h.1, bf16[768,128]{1,0:T(8,128)(2,1)} %k_h.1, ...), custom_call_target="tpu_custom_call" | custom-call | tf_op jit(solution)/shard_map/pallas_call | solution.py:641
  108.3 1.8 %copy.17 = bf16[768,256]{1,0:T(8,128)(2,1)} copy(bf16[768,256]{1,0:T(8,128)(2,1)} %shard_map.145) | data formatting | bytes 786432
